TPU v7x, 32 devices: a whole 2x2x4 slice. The times are simulated.
32 devices in a mesh: rep: 2 (over y), fs: 4 (over z), tp: 4 (over x, core).
Axes of the slice: x: 2, y: 2, z: 4, core: 2. Of those that a mesh axis runs over, the one named last changes fastest.
Arguments:
- activations: bfloat16 [8, 256, 2048], P(('rep', 'fs'), None, 'tp'), may hold values from -15 to 15
- norm_gain: float32 [2048], replicated, may hold values from 0.1 to 1.9
- w_value: bfloat16 [2048, 2048], P('fs', 'tp'), may hold values from -0.125 to 0.125
- w_gate_conv: bfloat16 [2048, 2048], P('fs', 'tp'), may hold values from -0.125 to 0.125
- conv_weight: float32 [31, 2048], P(None, 'tp'), may hold values from -3 to 3
- chan_gain: float32 [2048], P('tp'), may hold values from 0.1 to 1.9
- w_conv_out: bfloat16 [2048, 2048], P('tp', 'fs'), may hold values from -0.125 to 0.125
- mix_gain: float32 [2048], replicated, may hold values from 0.1 to 1.9
- w_gate: bfloat16 [2048, 3072], P('fs', 'tp'), may hold values from -0.125 to 0.125
- w_up: bfloat16 [2048, 3072], P('fs', 'tp'), may hold values from -0.125 to 0.125
- w_down: bfloat16 [3072, 2048], P('tp', 'fs'), may hold values from -0.109375 to 0.109375
- final_gain: float32 [2048], P('tp'), may hold values from 0.1 to 1.9
Outputs:
- result: bfloat16 [8, 256, 2048], P(('rep', 'fs'), None, 'tp')
All inputs are finite; a program needn't handle non-finite values.
Results may differ from a plain program's by a relative error of at most 0.013.
Values may be sent and summed in bfloat16 or wider, within the bound.
A program may use at most 64 MiB of HBM per device.

v0:
```python
import jax
import jax.numpy as jnp
from jax import lax
from jax.sharding import PartitionSpec as P

EPS = 1e-06


def body(
    activations,
    norm_gain,
    w_value,
    w_gate_conv,
    conv_weight,
    chan_gain,
    w_conv_out,
    mix_gain,
    w_gate,
    w_up,
    w_down,
    final_gain,
):
    batch, length, local_width = activations.shape
    width = local_width * lax.axis_size("tp")
    count = batch * length
    residual = activations.reshape(count, local_width).astype(jnp.float32)
    raw_in = lax.all_gather(
        activations.reshape(count, local_width), "tp", axis=1, tiled=True
    ).astype(jnp.float32)
    in_mean = jnp.mean(raw_in * raw_in, axis=1, keepdims=True)
    rows_in = (raw_in * lax.rsqrt(in_mean + EPS) * norm_gain).astype(jnp.bfloat16)
    chan_local = w_value.shape[1]
    pieces = (
        lax.all_gather(w_value, "fs", axis=0, tiled=True),
        lax.all_gather(w_gate_conv, "fs", axis=0, tiled=True),
    )
    columns = rows_in
    value = jnp.dot(columns, pieces[0], preferred_element_type=jnp.float32)
    gate_conv = jnp.dot(columns, pieces[1], preferred_element_type=jnp.float32)
    glu = (value * jax.nn.sigmoid(gate_conv)).reshape(batch, length, chan_local)
    taps = conv_weight.shape[0]
    padded = jnp.pad(glu, ((0, 0), (taps - 1, 0), (0, 0)))
    conv = lax.conv_general_dilated(
        padded,
        conv_weight[:, None, :],
        (1,),
        "VALID",
        dimension_numbers=("NWC", "WIO", "NWC"),
        feature_group_count=chan_local,
        precision=lax.Precision.HIGHEST,
    ).reshape(count, chan_local)
    chan_total = chan_local * lax.axis_size("tp")
    mean = lax.psum(jnp.sum(conv, axis=1), "tp") / chan_total
    centered = conv - mean[:, None]
    spread = lax.psum(jnp.sum(centered * centered, axis=1), "tp") / chan_total
    act = jax.nn.silu(centered * lax.rsqrt(spread + EPS)[:, None] * chan_gain).astype(jnp.bfloat16)
    conv_terms = jnp.dot(
        act,
        lax.all_gather(w_conv_out, "fs", axis=1, tiled=True),
        preferred_element_type=jnp.float32,
    )
    conv_out = lax.psum_scatter(
        conv_terms.astype(jnp.bfloat16), "tp", scatter_dimension=1, tiled=True
    ).astype(jnp.float32)
    first = (residual + conv_out).astype(jnp.bfloat16)
    first_f = first.astype(jnp.float32)
    raw_mid = lax.all_gather(first, "tp", axis=1, tiled=True).astype(jnp.float32)
    mid_mean = jnp.mean(raw_mid * raw_mid, axis=1, keepdims=True)
    rows_mid = (raw_mid * lax.rsqrt(mid_mean + EPS) * mix_gain).astype(jnp.bfloat16)
    hidden_local = w_gate.shape[1]
    zero_hidden = jnp.zeros((count, hidden_local), jnp.float32)
    pieces = (
        lax.all_gather(w_gate, "fs", axis=0, tiled=True),
        lax.all_gather(w_up, "fs", axis=0, tiled=True),
    )
    columns = lax.slice_in_dim(rows_mid, 0, pieces[0].shape[0], axis=1)
    gate = zero_hidden + jnp.dot(columns, pieces[0], preferred_element_type=jnp.float32)
    up = zero_hidden + jnp.dot(columns, pieces[1], preferred_element_type=jnp.float32)
    hidden = (jax.nn.silu(gate) * up).astype(jnp.bfloat16)
    ff_terms = jnp.dot(
        hidden, lax.all_gather(w_down, "fs", axis=1, tiled=True), preferred_element_type=jnp.float32
    )
    ff_out = lax.psum_scatter(
        ff_terms.astype(jnp.bfloat16), "tp", scatter_dimension=1, tiled=True
    ).astype(jnp.float32)
    second = first_f + ff_out
    out_total = lax.psum(jnp.sum(second * second, axis=1), "tp")
    result = (second * lax.rsqrt(out_total / width + EPS)[:, None] * final_gain).astype(
        jnp.bfloat16
    )
    return result.reshape(batch, length, local_width)


def solution(mesh):
    in_specs = (
        P(("rep", "fs"), None, "tp"),
        P(),
        P("fs", "tp"),
        P("fs", "tp"),
        P(None, "tp"),
        P("tp"),
        P("tp", "fs"),
        P(),
        P("fs", "tp"),
        P("fs", "tp"),
        P("tp", "fs"),
        P("tp"),
    )
    out_specs = P(("rep", "fs"), None, "tp")
    return jax.shard_map(body, mesh=mesh, in_specs=in_specs, out_specs=out_specs, check_vma=False)
```

profile of v0, /device:TPU:0, one launch (start us, length us, event | category | flops | bytes accessed | tf_op | source)
XLA Modules:
  0.0 451.0 jit_solution(17801474472369738869)
XLA Ops:
  6.5 0.7 all-gather.24.cloned.1.call-update
  7.3 0.0 all-gather.12.cloned.1.call-start
  7.3 0.7 all-gather.12.cloned.1.call-update
  8.0 0.0 all-gather.10.cloned.1.call-start
  8.1 0.7 all-gather.10.cloned.1.call-update
  8.7 0.0 all-gather.14.cloned.1.call-start
  8.8 0.5 all-gather.14.cloned.1.call-update
  9.3 0.0 reduce-scatter.3.cloned.1.call-start
  9.4 19.0 %all-gather.24.cloned.1.call-done = bf16[1,256,2048]{2,1,0:T(8,128)(2,1)} async-done(((bf16[1,256,512]{2,1,0:T(8,128)(2,1)}), bf16[1,256,2048]{2,1,0:T(8,128)(2,1)}) %all-gather.24.cloned.1.call-update) | async-done | bytes 1048592 | tf_op jit(solution)/shard_map/all_gather | solution.py:27
  28.4 1.5 fusion.3
  29.9 45.7 %all-gather.12.cloned.1.call-done = bf16[2048,512]{1,0:T(8,128)(2,1)} async-done(((bf16[512,512]{1,0:T(8,128)(2,1)}), bf16[2048,512]{1,0:T(8,128)(2,1)}) %all-gather.12.cloned.1.call-update) | async-done | bytes 2097168 | tf_op jit(solution)/shard_map/all_gather | solution.py:35
  75.6 2.8 fusion.10
  78.4 43.3 %all-gather.10.cloned.1.call-done = bf16[2048,512]{1,0:T(8,128)(2,1)} async-done(((bf16[512,512]{1,0:T(8,128)(2,1)}), bf16[2048,512]{1,0:T(8,128)(2,1)}) %all-gather.10.cloned.1.call-update) | async-done | bytes 2097168 | tf_op jit(solution)/shard_map/all_gather | solution.py:34
  121.7 2.3 fusion.7
  124.0 0.1 pad.2
  124.1 0.7 reshape.42
  124.8 0.2 copy.18
  125.0 0.1 slice.2
  125.1 1.2 convolution_select_fusion
  126.3 0.3 copy.20
  126.7 0.1 reshape.46
  126.8 0.1 slice_reduce_fusion
  126.9 6.4 %psum.21 = f32[256]{0:T(256)S(1)} all-reduce(f32[256]{0:T(256)S(1)} %slice_reduce_fusion), channel_id=1, replica_groups=mesh['rep'=2,'fs'=4,'tp'=4] {'tp'}, use_global_device_ids=true, to_apply=%region_2.3 | all-reduce | flops 256 | bytes 2048 | tf_op jit(solution)/shard_map/psum | solution.py:53
  133.3 0.2 multiply_reduce_fusion.1
  133.5 6.3 %psum.22 = f32[256]{0:T(256)S(1)} all-reduce(f32[256]{0:T(256)S(1)} %multiply_reduce_fusion.1), channel_id=1, replica_groups=mesh['rep'=2,'fs'=4,'tp'=4] {'tp'}, use_global_device_ids=true, to_apply=%region_4.5 | all-reduce | flops 256 | bytes 2048 | tf_op jit(solution)/shard_map/psum | solution.py:55
  139.8 27.8 %all-gather.14.cloned.1.call-done = bf16[512,2048]{1,0:T(8,128)(2,1)} async-done(((bf16[512,512]{1,0:T(8,128)(2,1)}), bf16[512,2048]{1,0:T(8,128)(2,1)}) %all-gather.14.cloned.1.call-update) | async-done | bytes 2097168 | tf_op jit(solution)/shard_map/all_gather | solution.py:59
  167.6 3.4 convolution_convert_fusion
  171.1 0.0 all-gather.16.cloned.1.call-start
  171.1 23.7 %reduce-scatter.3.cloned.1.call-done = bf16[256,512]{1,0:T(8,128)(2,1)} async-done(((bf16[256,2048]{1,0:T(8,128)(2,1)}), bf16[256,512]{1,0:T(8,128)(2,1)}) %reduce-scatter.3.cloned.1.call-update) | async-done | bytes 262160 | tf_op jit(solution)/shard_map/reduce_scatter | solution.py:62
  194.8 1.7 fusion.17
  196.6 0.0 all-gather.18.cloned.1.call-start
  196.6 0.7 all-gather.18.cloned.1.call-update
  197.3 0.0 all-gather.20.cloned.1.call-start
  197.4 0.7 all-gather.20.cloned.1.call-update
  198.1 0.0 all-gather.22.cloned.1.call-start
  198.1 0.7 all-gather.22.cloned.1.call-update
  198.8 0.0 reduce-scatter.5.cloned.1.call-start
  198.8 14.6 %all-gather.16.cloned.1.call-done = bf16[256,2048]{1,0:T(8,128)(2,1)} async-done(((bf16[256,512]{1,0:T(8,128)(2,1)}), bf16[256,2048]{1,0:T(8,128)(2,1)}) %all-gather.16.cloned.1.call-update) | async-done | bytes 1048592 | tf_op jit(solution)/shard_map/all_gather | solution.py:67
  213.4 1.5 fusion
  215.0 63.5 %all-gather.18.cloned.1.call-done = bf16[2048,768]{1,0:T(8,128)(2,1)} async-done(((bf16[512,768]{1,0:T(8,128)(2,1)}), bf16[2048,768]{1,0:T(8,128)(2,1)}) %all-gather.18.cloned.1.call-update) | async-done | bytes 3145744 | tf_op jit(solution)/shard_map/all_gather | solution.py:73
  278.5 3.2 fusion.23
  281.8 60.4 %all-gather.20.cloned.1.call-done = bf16[2048,768]{1,0:T(8,128)(2,1)} async-done(((bf16[512,768]{1,0:T(8,128)(2,1)}), bf16[2048,768]{1,0:T(8,128)(2,1)}) %all-gather.20.cloned.1.call-update) | async-done | bytes 3145744 | tf_op jit(solution)/shard_map/all_gather | solution.py:74
  342.2 63.7 %all-gather.22.cloned.1.call-done = bf16[768,2048]{1,0:T(8,128)(2,1)} async-done(((bf16[768,512]{1,0:T(8,128)(2,1)}), bf16[768,2048]{1,0:T(8,128)(2,1)}) %all-gather.22.cloned.1.call-update) | async-done | bytes 3145744 | tf_op jit(solution)/shard_map/all_gather | solution.py:81
  405.9 6.0 %convolution_convert_fusion.1 = bf16[256,2048]{1,0:T(8,128)(2,1)} fusion(bf16[768,2048]{1,0:T(8,128)(2,1)} %all-gather.22.cloned.1.call-done, bf16[2048,768]{1,0:T(8,128)(2,1)} %all-gather.20.cloned.1.call-done, f32[256,768]{1,0:T(8,128)S(1)} %fusion.23, bf16[256,2048]{1,0:T(8,128)(2,1)S(1)} %copy-done.3, f32[2048]{0:T(1024)S(1)} %copy-done.7, ...), kind=kOutput, calls=%fused_computation.5 | convolution fusion | flops 1614413824 | bytes 9184256 | tf_op jit(solution)/shard_map/dot_general | solution.py:80
  411.9 23.6 %reduce-scatter.5.cloned.1.call-done = bf16[256,512]{1,0:T(8,128)(2,1)} async-done(((bf16[256,2048]{1,0:T(8,128)(2,1)}), bf16[256,512]{1,0:T(8,128)(2,1)}) %reduce-scatter.5.cloned.1.call-update) | async-done | bytes 262160 | tf_op jit(solution)/shard_map/reduce_scatter | solution.py:83
  435.5 1.1 multiply_reduce_fusion
  436.6 5.8 %psum.23 = f32[256]{0:T(256)S(1)} all-reduce(f32[256]{0:T(256)S(1)} %multiply_reduce_fusion), channel_id=1, replica_groups=mesh['rep'=2,'fs'=4,'tp'=4] {'tp'}, use_global_device_ids=true, to_apply=%region_9.10 | all-reduce | flops 256 | bytes 2048 | tf_op jit(solution)/shard_map/psum | solution.py:87
  442.4 1.8 fusion.25
  (29 shorter events, 0.1 us)
Async XLA Ops:
  6.5 118.5 %copy-start = (f32[31,512]{1,0:T(8,128)S(1)}, f32[31,512]{1,0:T(8,128)}, u32[]{:S(2)}) copy-start(f32[31,512]{1,0:T(8,128)} %param.16) | copy-start | bytes 190468
  6.5 69.1 %copy-start.6 = (f32[2048]{0:T(1024)S(1)}, f32[2048]{0:T(1024)}, u32[]{:S(2)}) copy-start(f32[2048]{0:T(1024)} %param.13) | copy-start | bytes 24580
  6.5 21.8 %all-gather.24.cloned.1.call-start = ((), (), s32[]{:S(2)}) async-start(), calls=%async_computation.11 | async-start | bytes 1310720 | tf_op jit(solution)/shard_map/all_gather | solution.py:27
  7.3 68.3 %all-gather.12.cloned.1.call-start = ((), (), s32[]{:S(2)}) async-start(), calls=%async_computation.3 | async-start | bytes 2621440 | tf_op jit(solution)/shard_map/all_gather | solution.py:35
  8.0 113.7 %all-gather.10.cloned.1.call-start = ((), (), s32[]{:S(2)}) async-start(), calls=%async_computation.2 | async-start | bytes 2621440 | tf_op jit(solution)/shard_map/all_gather | solution.py:34
  8.7 158.9 %all-gather.14.cloned.1.call-start = ((), (), s32[]{:S(2)}) async-start(), calls=%async_computation.4 | async-start | bytes 2621440 | tf_op jit(solution)/shard_map/all_gather | solution.py:59
  9.3 185.5 %reduce-scatter.3.cloned.1.call-start = ((), (), s32[]{:S(2)}) async-start(), calls=%async_computation.5 | async-start | bytes 1310720 | tf_op jit(solution)/shard_map/reduce_scatter | solution.py:62
  29.9 91.8 %copy-start.4 = (bf16[1,256,2048]{2,1,0:T(8,128)(2,1)S(1)}, bf16[1,256,2048]{2,1,0:T(8,128)(2,1)}, u32[]{:S(2)}) copy-start(bf16[1,256,2048]{2,1,0:T(8,128)(2,1)} %all-gather.24.cloned.1.call-done) | copy-start | bytes 3145732
  124.0 1.0 copy-start.9
  126.3 41.3 %copy-start.8 = (f32[512]{0:T(512)S(1)}, f32[512]{0:T(512)}, u32[]{:S(2)}) copy-start(f32[512]{0:T(512)} %param.17) | copy-start | bytes 6148
  139.8 55.1 %copy-start.2 = (bf16[1,256,512]{2,1,0:T(8,128)(2,1)S(1)}, bf16[1,256,512]{2,1,0:T(8,128)(2,1)}, u32[]{:S(2)}) copy-start(bf16[1,256,512]{2,1,0:T(8,128)(2,1)} %param.12) | copy-start | bytes 786436
  171.1 107.4 %copy-start.7 = (f32[2048]{0:T(1024)S(1)}, f32[2048]{0:T(1024)}, u32[]{:S(2)}) copy-start(f32[2048]{0:T(1024)} %param.19) | copy-start | bytes 24580
  171.1 42.4 %all-gather.16.cloned.1.call-start = ((), (), s32[]{:S(2)}) async-start(), calls=%async_computation.6 | async-start | bytes 1310720 | tf_op jit(solution)/shard_map/all_gather | solution.py:67
  196.6 81.9 %all-gather.18.cloned.1.call-start = ((), (), s32[]{:S(2)}) async-start(), calls=%async_computation.7 | async-start | bytes 3932160 | tf_op jit(solution)/shard_map/all_gather | solution.py:73
  197.3 144.8 %all-gather.20.cloned.1.call-start = ((), (), s32[]{:S(2)}) async-start(), calls=%async_computation.8 | async-start | bytes 3932160 | tf_op jit(solution)/shard_map/all_gather | solution.py:74
  198.1 207.8 %all-gather.22.cloned.1.call-start = ((), (), s32[]{:S(2)}) async-start(), calls=%async_computation.9 | async-start | bytes 3932160 | tf_op jit(solution)/shard_map/all_gather | solution.py:81
  198.8 236.7 %reduce-scatter.5.cloned.1.call-start = ((), (), s32[]{:S(2)}) async-start(), calls=%async_computation.10 | async-start | bytes 1310720 | tf_op jit(solution)/shard_map/reduce_scatter | solution.py:83
  214.9 190.9 %copy-start.3 = (bf16[256,2048]{1,0:T(8,128)(2,1)S(1)}, bf16[256,2048]{1,0:T(8,128)(2,1)}, u32[]{:S(2)}) copy-start(bf16[256,2048]{1,0:T(8,128)(2,1)} %all-gather.16.cloned.1.call-done) | copy-start | bytes 3145732
  281.7 153.8 %copy-start.1 = (bf16[256,512]{1,0:T(8,128)(2,1)S(1)}, bf16[256,512]{1,0:T(8,128)(2,1)}, u32[]{:S(2)}) copy-start(bf16[256,512]{1,0:T(8,128)(2,1)} %fusion.17) | copy-start | bytes 786436
  281.7 160.6 %copy-start.5 = (f32[512]{0:T(512)S(1)}, f32[512]{0:T(512)}, u32[]{:S(2)}) copy-start(f32[512]{0:T(512)} %param.23) | copy-start | bytes 6148
Sparse Core Ops, SparseCore 0:
  8.9 19.4 all-gather.23
  29.9 45.6 all-gather.11
  77.2 44.4 all-gather.9
  123.1 44.4 all-gather.13
  171.2 23.6 reduce-scatter.2
  196.7 16.6 all-gather.15
  215.0 63.4 all-gather.17
  280.0 62.0 all-gather.19
  343.7 62.0 all-gather.21
  412.0 23.4 reduce-scatter.4
where the time goes:
time: 451 us
  waiting for transfers between devices  390 us (86%)
  matrix products  19 us (4%)
  blocking collectives  18.4 us (4%)
  between operations  13.7 us (3%)
  other arithmetic  7.97 us (2%)
    all_gather x1, waiting for transfers between devices, body(): lax.all_gather(w_down, 'fs', axis=1, tiled=True)  63.7 us
    all_gather x1, waiting for transfers between devices, body(): lax.all_gather(w_gate, 'fs', axis=0, tiled=True)  63.5 us
    all_gather x1, waiting for transfers between devices, body(): lax.all_gather(w_up, 'fs', axis=0, tiled=True)  60.4 us
    all_gather x1, waiting for transfers between devices, body(): lax.all_gather(w_gate_conv, 'fs', axis=0, tiled=True)  45.7 us
    all_gather x1, waiting for transfers between devices, body(): lax.all_gather(w_value, 'fs', axis=0, tiled=True)  43.3 us
    all_gather x1, waiting for transfers between devices, body(): lax.all_gather(w_conv_out, 'fs', axis=1, tiled=True)  27.8 us
    reduce_scatter x1, waiting for transfers between devices, body(): lax.psum_scatter(conv_terms.astype(jnp.bfloat16), 'tp', scatter_dimension...  23.7 us
    reduce_scatter x1, waiting for transfers between devices, body(): lax.psum_scatter(ff_terms.astype(jnp.bfloat16), 'tp', scatter_dimension=1...  23.6 us
  transfers between devices with their start and end apart: 10, of which 10 were waited for; matrix products, arithmetic and copies ran while one was open for 3% of the time, Pallas kernels for 0%

commit v1 on v0

--- a/solution.py
+++ b/solution.py
@@ -20,6 +20,10 @@
     w_down,
     final_gain,
 ):
+
+    def test_spans_by_axis(obj, pos_dim):
+        return jnp.concatenate(lax.all_gather(obj, axis_name="fs"), axis=pos_dim)
+
     batch, length, local_width = activations.shape
     width = local_width * lax.axis_size("tp")
     count = batch * length
@@ -54,11 +58,7 @@
     centered = conv - mean[:, None]
     spread = lax.psum(jnp.sum(centered * centered, axis=1), "tp") / chan_total
     act = jax.nn.silu(centered * lax.rsqrt(spread + EPS)[:, None] * chan_gain).astype(jnp.bfloat16)
-    conv_terms = jnp.dot(
-        act,
-        lax.all_gather(w_conv_out, "fs", axis=1, tiled=True),
-        preferred_element_type=jnp.float32,
-    )
+    conv_terms = jnp.dot(act, test_spans_by_axis(w_conv_out, 1), preferred_element_type=jnp.float32)
     conv_out = lax.psum_scatter(
         conv_terms.astype(jnp.bfloat16), "tp", scatter_dimension=1, tiled=True
     ).astype(jnp.float32)

time: 451 us -> 453 us (level)
  no operation moved by 1% of the time
where the time goes in v1:
time: 453 us; the launch traced here: 452 us
  waiting for transfers between devices  390 us (86%)
  blocking collectives  18.4 us (4%)
  matrix products  17.4 us (4%)
  between operations  13.7 us (3%)
  other arithmetic  7.97 us (2%)
    all_gather x1, waiting for transfers between devices, body(): lax.all_gather(w_down, 'fs', axis=1, tiled=True)  63.7 us
    all_gather x1, waiting for transfers between devices, body(): lax.all_gather(w_gate, 'fs', axis=0, tiled=True)  63.5 us
    all_gather x1, waiting for transfers between devices, body(): lax.all_gather(w_up, 'fs', axis=0, tiled=True)  60.4 us
    all_gather x1, waiting for transfers between devices, body(): lax.all_gather(w_gate_conv, 'fs', axis=0, tiled=True)  45.7 us
    all_gather x1, waiting for transfers between devices, body(): lax.all_gather(w_value, 'fs', axis=0, tiled=True)  43.3 us
    all_gather x1, waiting for transfers between devices, test_spans_by_axis(): return jnp.concatenate(lax.all_gather(obj, axis_name='fs'), axis=pos_dim)  27.9 us
    reduce_scatter x1, waiting for transfers between devices, body(): lax.psum_scatter(conv_terms.astype(jnp.bfloat16), 'tp', scatter_dimension...  23.7 us
    reduce_scatter x1, waiting for transfers between devices, body(): lax.psum_scatter(ff_terms.astype(jnp.bfloat16), 'tp', scatter_dimension=1...  23.6 us
  transfers between devices with their start and end apart: 10, of which 10 were waited for; matrix products, arithmetic and copies ran while one was open for 3% of the time, Pallas kernels for 0%

profile of v1, /device:TPU:0, one launch (start us, length us, event | category | flops | bytes accessed | tf_op | source)
XLA Modules:
  0.0 452.2 jit_solution(11743184909991592886)
XLA Ops:
  6.5 0.7 all-gather.23.cloned.1.call-update
  7.3 0.0 all-gather.13.cloned.1.call-start
  7.3 0.7 all-gather.13.cloned.1.call-update
  8.0 0.0 all-gather.11.cloned.1.call-start
  8.1 0.7 all-gather.11.cloned.1.call-update
  8.7 0.0 all-gather.25.cloned.1.call-start
  8.8 0.5 all-gather.25.cloned.1.call-update
  9.3 0.0 reduce-scatter.3.cloned.1.call-start
  9.4 19.0 %all-gather.23.cloned.1.call-done = bf16[1,256,2048]{2,1,0:T(8,128)(2,1)} async-done(((bf16[1,256,512]{2,1,0:T(8,128)(2,1)}), bf16[1,256,2048]{2,1,0:T(8,128)(2,1)}) %all-gather.23.cloned.1.call-update) | async-done | bytes 1048592 | tf_op jit(solution)/shard_map/all_gather | solution.py:31
  28.4 1.5 fusion.3
  29.9 45.7 %all-gather.13.cloned.1.call-done = bf16[2048,512]{1,0:T(8,128)(2,1)} async-done(((bf16[512,512]{1,0:T(8,128)(2,1)}), bf16[2048,512]{1,0:T(8,128)(2,1)}) %all-gather.13.cloned.1.call-update) | async-done | bytes 2097168 | tf_op jit(solution)/shard_map/all_gather | solution.py:39
  75.6 2.8 fusion.10
  78.4 43.3 %all-gather.11.cloned.1.call-done = bf16[2048,512]{1,0:T(8,128)(2,1)} async-done(((bf16[512,512]{1,0:T(8,128)(2,1)}), bf16[2048,512]{1,0:T(8,128)(2,1)}) %all-gather.11.cloned.1.call-update) | async-done | bytes 2097168 | tf_op jit(solution)/shard_map/all_gather | solution.py:38
  121.7 2.3 fusion.7
  124.0 0.1 pad.2
  124.1 0.7 reshape.67
  124.8 0.2 copy.21
  125.0 0.1 slice.2
  125.1 1.2 convolution_select_fusion
  126.3 0.3 copy.23
  126.7 0.1 reshape.71
  126.7 0.1 slice_reduce_fusion
  126.9 6.4 %psum.21 = f32[256]{0:T(256)S(1)} all-reduce(f32[256]{0:T(256)S(1)} %slice_reduce_fusion), channel_id=1, replica_groups=mesh['rep'=2,'fs'=4,'tp'=4] {'tp'}, use_global_device_ids=true, to_apply=%region_2.3 | all-reduce | flops 256 | bytes 2048 | tf_op jit(solution)/shard_map/psum | solution.py:57
  133.3 0.2 fusion.19
  133.5 6.3 %psum.22 = f32[256]{0:T(256)S(1)} all-reduce(f32[256]{0:T(256)S(1)} %fusion.19), channel_id=1, replica_groups=mesh['rep'=2,'fs'=4,'tp'=4] {'tp'}, use_global_device_ids=true, to_apply=%region_4.5 | all-reduce | flops 256 | bytes 2048 | tf_op jit(solution)/shard_map/psum | solution.py:59
  139.7 27.9 %all-gather.25.cloned.1.call-done = bf16[2048,512]{1,0:T(8,128)(2,1)} async-done(((bf16[512,512]{1,0:T(8,128)(2,1)}), bf16[2048,512]{1,0:T(8,128)(2,1)}) %all-gather.25.cloned.1.call-update) | async-done | bytes 2097168 | tf_op jit(solution)/shard_map/all_gather | solution.py:25
  167.6 2.8 copy.24
  170.4 1.8 convolution_convert_fusion
  172.3 0.0 all-gather.15.cloned.1.call-start
  172.3 23.7 %reduce-scatter.3.cloned.1.call-done = bf16[256,512]{1,0:T(8,128)(2,1)} async-done(((bf16[256,2048]{1,0:T(8,128)(2,1)}), bf16[256,512]{1,0:T(8,128)(2,1)}) %reduce-scatter.3.cloned.1.call-update) | async-done | bytes 262160 | tf_op jit(solution)/shard_map/reduce_scatter | solution.py:62
  196.0 1.7 fusion.17
  197.8 0.0 all-gather.17.cloned.1.call-start
  197.8 0.7 all-gather.17.cloned.1.call-update
  198.6 0.7 all-gather.19.cloned.1.call-update
  199.3 0.0 all-gather.21.cloned.1.call-start
  199.3 0.7 all-gather.21.cloned.1.call-update
  200.0 0.0 reduce-scatter.5.cloned.1.call-start
  200.0 14.6 %all-gather.15.cloned.1.call-done = bf16[256,2048]{1,0:T(8,128)(2,1)} async-done(((bf16[256,512]{1,0:T(8,128)(2,1)}), bf16[256,2048]{1,0:T(8,128)(2,1)}) %all-gather.15.cloned.1.call-update) | async-done | bytes 1048592 | tf_op jit(solution)/shard_map/all_gather | solution.py:67
  214.6 1.5 fusion
  216.1 63.5 %all-gather.17.cloned.1.call-done = bf16[2048,768]{1,0:T(8,128)(2,1)} async-done(((bf16[512,768]{1,0:T(8,128)(2,1)}), bf16[2048,768]{1,0:T(8,128)(2,1)}) %all-gather.17.cloned.1.call-update) | async-done | bytes 3145744 | tf_op jit(solution)/shard_map/all_gather | solution.py:73
  279.7 3.2 fusion.25
  282.9 60.4 %all-gather.19.cloned.1.call-done = bf16[2048,768]{1,0:T(8,128)(2,1)} async-done(((bf16[512,768]{1,0:T(8,128)(2,1)}), bf16[2048,768]{1,0:T(8,128)(2,1)}) %all-gather.19.cloned.1.call-update) | async-done | bytes 3145744 | tf_op jit(solution)/shard_map/all_gather | solution.py:74
  343.3 63.7 %all-gather.21.cloned.1.call-done = bf16[768,2048]{1,0:T(8,128)(2,1)} async-done(((bf16[768,512]{1,0:T(8,128)(2,1)}), bf16[768,2048]{1,0:T(8,128)(2,1)}) %all-gather.21.cloned.1.call-update) | async-done | bytes 3145744 | tf_op jit(solution)/shard_map/all_gather | solution.py:81
  407.0 6.0 %convolution_convert_fusion.1 = bf16[256,2048]{1,0:T(8,128)(2,1)} fusion(bf16[768,2048]{1,0:T(8,128)(2,1)} %all-gather.21.cloned.1.call-done, bf16[2048,768]{1,0:T(8,128)(2,1)} %all-gather.19.cloned.1.call-done, f32[256,768]{1,0:T(8,128)S(1)} %fusion.25, bf16[256,2048]{1,0:T(8,128)(2,1)S(1)} %copy-done.3, f32[2048]{0:T(1024)S(1)} %copy-done.7, ...), kind=kOutput, calls=%fused_computation.5 | convolution fusion | flops 1614413824 | bytes 9184256 | tf_op jit(solution)/shard_map/dot_general | solution.py:80
  413.1 23.6 %reduce-scatter.5.cloned.1.call-done = bf16[256,512]{1,0:T(8,128)(2,1)} async-done(((bf16[256,2048]{1,0:T(8,128)(2,1)}), bf16[256,512]{1,0:T(8,128)(2,1)}) %reduce-scatter.5.cloned.1.call-update) | async-done | bytes 262160 | tf_op jit(solution)/shard_map/reduce_scatter | solution.py:83
  436.7 1.1 multiply_reduce_fusion
  437.8 5.8 %psum.23 = f32[256]{0:T(256)S(1)} all-reduce(f32[256]{0:T(256)S(1)} %multiply_reduce_fusion), channel_id=1, replica_groups=mesh['rep'=2,'fs'=4,'tp'=4] {'tp'}, use_global_device_ids=true, to_apply=%region_9.10 | all-reduce | flops 256 | bytes 2048 | tf_op jit(solution)/shard_map/psum | solution.py:87
  443.6 1.8 fusion.27
  (30 shorter events, 0.2 us)
Async XLA Ops:
  6.5 118.5 %copy-start = (f32[31,512]{1,0:T(8,128)S(1)}, f32[31,512]{1,0:T(8,128)}, u32[]{:S(2)}) copy-start(f32[31,512]{1,0:T(8,128)} %param.16) | copy-start | bytes 190468
  6.5 69.1 %copy-start.6 = (f32[2048]{0:T(1024)S(1)}, f32[2048]{0:T(1024)}, u32[]{:S(2)}) copy-start(f32[2048]{0:T(1024)} %param.13) | copy-start | bytes 24580
  6.5 21.8 %all-gather.23.cloned.1.call-start = ((), (), s32[]{:S(2)}) async-start(), calls=%async_computation.10 | async-start | bytes 1310720 | tf_op jit(solution)/shard_map/all_gather | solution.py:31
  7.3 68.3 %all-gather.13.cloned.1.call-start = ((), (), s32[]{:S(2)}) async-start(), calls=%async_computation.3 | async-start | bytes 2621440 | tf_op jit(solution)/shard_map/all_gather | solution.py:39
  8.0 113.7 %all-gather.11.cloned.1.call-start = ((), (), s32[]{:S(2)}) async-start(), calls=%async_computation.2 | async-start | bytes 2621440 | tf_op jit(solution)/shard_map/all_gather | solution.py:38
  8.7 158.9 %all-gather.25.cloned.1.call-start = ((), (), s32[]{:S(2)}) async-start(), calls=%async_computation.11 | async-start | bytes 2621440 | tf_op jit(solution)/shard_map/all_gather | solution.py:25
  9.3 186.7 %reduce-scatter.3.cloned.1.call-start = ((), (), s32[]{:S(2)}) async-start(), calls=%async_computation.4 | async-start | bytes 1310720 | tf_op jit(solution)/shard_map/reduce_scatter | solution.py:62
  29.9 91.8 %copy-start.4 = (bf16[1,256,2048]{2,1,0:T(8,128)(2,1)S(1)}, bf16[1,256,2048]{2,1,0:T(8,128)(2,1)}, u32[]{:S(2)}) copy-start(bf16[1,256,2048]{2,1,0:T(8,128)(2,1)} %all-gather.23.cloned.1.call-done) | copy-start | bytes 3145732
  124.0 1.0 copy-start.9
  167.6 2.8 copy-start.8
  170.4 25.6 %copy-start.2 = (bf16[1,256,512]{2,1,0:T(8,128)(2,1)S(1)}, bf16[1,256,512]{2,1,0:T(8,128)(2,1)}, u32[]{:S(2)}) copy-start(bf16[1,256,512]{2,1,0:T(8,128)(2,1)} %param.12) | copy-start | bytes 786436
  172.3 107.4 %copy-start.7 = (f32[2048]{0:T(1024)S(1)}, f32[2048]{0:T(1024)}, u32[]{:S(2)}) copy-start(f32[2048]{0:T(1024)} %param.19) | copy-start | bytes 24580
  172.3 42.3 %all-gather.15.cloned.1.call-start = ((), (), s32[]{:S(2)}) async-start(), calls=%async_computation.5 | async-start | bytes 1310720 | tf_op jit(solution)/shard_map/all_gather | solution.py:67
  197.8 81.9 %all-gather.17.cloned.1.call-start = ((), (), s32[]{:S(2)}) async-start(), calls=%async_computation.6 | async-start | bytes 3932160 | tf_op jit(solution)/shard_map/all_gather | solution.py:73
  198.5 144.8 %all-gather.19.cloned.1.call-start = ((), (), s32[]{:S(2)}) async-start(), calls=%async_computation.7 | async-start | bytes 3932160 | tf_op jit(solution)/shard_map/all_gather | solution.py:74
  199.3 207.8 %all-gather.21.cloned.1.call-start = ((), (), s32[]{:S(2)}) async-start(), calls=%async_computation.8 | async-start | bytes 3932160 | tf_op jit(solution)/shard_map/all_gather | solution.py:81
  200.0 236.7 %reduce-scatter.5.cloned.1.call-start = ((), (), s32[]{:S(2)}) async-start(), calls=%async_computation.9 | async-start | bytes 1310720 | tf_op jit(solution)/shard_map/reduce_scatter | solution.py:83
  216.1 190.9 %copy-start.3 = (bf16[256,2048]{1,0:T(8,128)(2,1)S(1)}, bf16[256,2048]{1,0:T(8,128)(2,1)}, u32[]{:S(2)}) copy-start(bf16[256,2048]{1,0:T(8,128)(2,1)} %all-gather.15.cloned.1.call-done) | copy-start | bytes 3145732
  282.9 153.8 %copy-start.1 = (bf16[256,512]{1,0:T(8,128)(2,1)S(1)}, bf16[256,512]{1,0:T(8,128)(2,1)}, u32[]{:S(2)}) copy-start(bf16[256,512]{1,0:T(8,128)(2,1)} %fusion.17) | copy-start | bytes 786436
  282.9 160.6 %copy-start.5 = (f32[512]{0:T(512)S(1)}, f32[512]{0:T(512)}, u32[]{:S(2)}) copy-start(f32[512]{0:T(512)} %param.23) | copy-start | bytes 6148
Sparse Core Ops, SparseCore 0:
  8.9 19.4 all-gather.22
  29.9 45.6 all-gather.12
  77.2 44.4 all-gather.10
  123.1 44.4 all-gather.24
  172.4 23.5 reduce-scatter.2
  197.9 16.6 all-gather.14
  216.2 63.4 all-gather.16
  281.2 62.0 all-gather.18
  344.9 62.0 all-gather.20
  413.2 23.4 reduce-scatter.4
